TPU v7x, 32 devices: a whole 2x2x4 slice. The times are simulated.
32 devices in a mesh: gr: 2 (over core), sp: 8 (over z, y), tp: 2 (over x).
Axes of the slice: x: 2, y: 2, z: 4, core: 2. Of those that a mesh axis runs over, the one named last changes fastest.
Arguments:
- tokens: bfloat16 [4, 2048, 2048], P('gr', ('sp', 'tp')), parts along dimension 0, may hold values from -6 to 6
- key_weight: bfloat16 [2048, 1024], P('sp'), may hold values from -0.125 to 0.125
- value_weight: bfloat16 [2048, 1024], P('sp'), may hold values from -0.125 to 0.125
- queries: bfloat16 [4, 1024], P('gr'), parts along dimension 0, may hold values from -6 to 6
- head_offset: float32 [16], replicated, may hold values from -14 to -3.5
- key_bias: bfloat16 [4, 2048, 16], P('gr', ('sp', 'tp')), parts along dimension 0, may hold values from -0.5 to 12.9
Outputs:
- key_cache: bfloat16 [4, 2048, 1024], P('gr', 'sp', 'tp'), parts along dimension 0
- value_cache: bfloat16 [4, 2048, 1024], P('gr', 'sp', 'tp'), parts along dimension 0
- bias_cache: bfloat16 [4, 2048, 16], P('gr', 'sp', 'tp'), parts along dimension 0
- reading: float32 [4, 1024], P('gr', 'tp'), parts along dimension 0
There are 2 independent parts, one for each index of `gr`. A program takes and returns all parts, laid end to end along the dimension named above; an argument that names none is the same for every part. Nothing has to cross between parts.
All inputs are finite; a program needn't handle non-finite values.
Results may differ from a plain program's by a relative error of at most 0.0052.
Values may be sent and summed in bfloat16 or wider, within the bound.
A program may use at most 64 MiB of HBM per device.

v0:
```python
import jax
import jax.numpy as jnp
from jax import lax
from jax.sharding import PartitionSpec as P


def carried_in(x, axis, combine, identity):
    length, position = (lax.axis_size(axis), lax.axis_index(axis))
    everything = lax.all_gather(x, axis)
    start = jnp.broadcast_to(jnp.asarray(identity, x.dtype), x.shape)

    def lap(k, before):
        at = length - 1 - k
        reached = at > position
        new = combine(before, everything[at])
        return jnp.where(reached, new, before)

    return lax.fori_loop(0, length, lap, start)


def add_terms(earlier, later):
    return earlier + later


def normalize(mixture):
    return mixture * lax.rsqrt(jnp.mean(mixture * mixture, axis=-1, keepdims=True) + 1e-06)


def per_device(tokens, key_weight, value_weight, queries, head_offset, key_bias):
    seq_count, pos_dev, model_width = tokens.shape
    head_count = head_offset.shape[0]
    kv_width = key_weight.shape[1]
    head_dim = kv_width // head_count
    score_scale = head_dim ** (-0.5)
    tp_count = lax.axis_size("tp")
    col_width = kv_width // tp_count
    col_start = lax.axis_index("tp") * col_width
    own_cols = jnp.concatenate(
        [
            lax.dynamic_slice_in_dim(key_weight, col_start, col_width, 1),
            lax.dynamic_slice_in_dim(value_weight, col_start, col_width, 1),
        ],
        axis=1,
    )
    full_cols = lax.all_gather(own_cols, "sp", axis=0, tiled=True)
    projected = jnp.einsum(
        "spd,dw->spw",
        lax.all_gather(tokens, "tp", axis=1, tiled=True),
        full_cols,
        preferred_element_type=jnp.float32,
    ).astype(jnp.bfloat16)
    key_cache = projected[:, :, :col_width]
    value_cache = projected[:, :, col_width:]
    bias_cache = lax.all_to_all(key_bias, "tp", split_axis=2, concat_axis=1, tiled=True)
    span_len = key_cache.shape[1]
    local_heads = bias_cache.shape[2]
    key_blocks = key_cache.reshape(seq_count, span_len, local_heads, head_dim)
    value_blocks = value_cache.reshape(seq_count, span_len, local_heads, head_dim)
    query_cols = lax.dynamic_slice_in_dim(queries, col_start, col_width, 1)
    query_heads = query_cols.reshape(seq_count, local_heads, head_dim)
    head_start = lax.axis_index("tp") * local_heads
    local_offset = lax.dynamic_slice_in_dim(head_offset, head_start, local_heads, 0)
    logits = (
        jnp.einsum("sphc,shc->shp", key_blocks, query_heads, preferred_element_type=jnp.float32)
        * score_scale
    )
    logits = (
        logits
        + local_offset[None, :, None]
        + jnp.transpose(bias_cache.astype(jnp.float32), (0, 2, 1))
    )
    fading = jax.nn.log_sigmoid(-logits)
    within = lax.cumsum(fading, axis=2, reverse=True) - fading
    block_total = jnp.sum(fading, axis=2)
    carried = carried_in(block_total, "sp", add_terms, jnp.zeros_like(block_total))
    weights = jnp.exp(jax.nn.log_sigmoid(logits) + within + carried[:, :, None]).astype(
        jnp.bfloat16
    )
    partial_value = jnp.einsum(
        "shp,sphc->shc", weights, value_blocks, preferred_element_type=jnp.float32
    )
    mixture = lax.psum(partial_value, "sp")
    reading = normalize(mixture).reshape(seq_count, col_width)
    return (key_cache, value_cache, bias_cache, reading)


def solution(mesh):
    in_specs = (
        P("gr", ("sp", "tp"), None),
        P("sp", None),
        P("sp", None),
        P("gr", None),
        P(),
        P("gr", ("sp", "tp"), None),
    )
    out_specs = (P("gr", "sp", "tp"), P("gr", "sp", "tp"), P("gr", "sp", "tp"), P("gr", "tp"))
    return jax.shard_map(
        per_device, mesh=mesh, in_specs=in_specs, out_specs=out_specs, check_vma=False
    )
```

profile of v0, /device:TPU:0, one launch (start us, length us, event | category | flops | bytes accessed | tf_op | source)
XLA Modules:
  0.0 179.6 jit_solution(294673093222609058)
XLA Ops:
  7.2 0.0 copy-start
  7.2 0.0 all-gather.7.cloned.1.call-start
  7.2 0.7 all-gather.7.cloned.1.call-update
  7.9 0.0 copy-start.2
  7.9 0.0 copy-start.3
  7.9 0.0 all-gather.5.cloned.1.call-start
  8.0 1.1 constant_dynamic-slice_fusion.1
  9.1 0.1 copy.28
  9.2 0.1 copy.29
  9.3 0.8 pad_maximum_fusion
  10.2 0.0 all-gather.5.cloned.1.call-update
  10.2 0.0 copy-done.2
  10.2 0.6 copy.20
  10.8 4.2 %all-to-all-start = ((bf16[2,128,16]{1,0,2:T(2,128)(2,1)}), bf16[2,128,16]{1,0,2:T(2,128)(2,1)S(1)}, u32[]{:S(2)}, u32[]{:S(2)}) async-start(bf16[2,128,16]{1,0,2:T(2,128)(2,1)} %copy.20), calls=%async_computation | async-start | bytes 16384 | tf_op jit(solution)/shard_map/all_to_all | solution.py:54
  15.0 0.0 copy-done
  15.1 0.1 reshape.64
  15.1 0.0 copy-done.3
  15.1 0.1 dynamic_slice.25
  15.2 30.2 %all-gather.7.cloned.1.call-done = bf16[2,256,2048]{2,1,0:T(8,128)(2,1)} async-done(((bf16[2,128,2048]{2,1,0:T(8,128)(2,1)}), bf16[2,256,2048]{2,1,0:T(8,128)(2,1)}) %all-gather.7.cloned.1.call-update) | async-done | bytes 2097168 | tf_op jit(solution)/shard_map/all_gather | solution.py:48
  45.4 77.3 %all-gather.5.cloned.1.call-done = bf16[2048,1024]{0,1:T(8,128)(2,1)} async-done(((bf16[256,1024]{0,1:T(8,128)(2,1)}), bf16[2048,1024]{0,1:T(8,128)(2,1)}) %all-gather.5.cloned.1.call-update) | async-done | bytes 4194320 | tf_op jit(solution)/shard_map/all_gather | solution.py:45
  122.7 5.2 %fusion.5 = bf16[2,256,1024]{1,2,0:T(8,128)(2,1)S(1)} fusion(bf16[2,256,2048]{2,1,0:T(8,128)(2,1)} %all-gather.7.cloned.1.call-done, bf16[2048,1024]{0,1:T(8,128)(2,1)} %all-gather.5.cloned.1.call-done), kind=kOutput, calls=%fused_computation.4 | convolution fusion | flops 2148007936 | bytes 7340032 | tf_op jit(solution)/shard_map/spd,dw->spw/dot_general | solution.py:46
  127.9 0.1 fusion.18
  128.0 0.2 fusion.19
  128.2 1.0 copy.22
  129.2 0.0 all-to-all-done
  129.2 0.1 negate_bitcast_fusion
  129.3 0.0 copy-start.1
  129.3 0.2 fusion.16
  129.5 17.7 %all-gather.1 = f32[8,2,8]{2,1,0:T(2,128)S(1)} all-gather(f32[1,2,8]{2,1,0:T(2,128)S(1)} %negate_bitcast_fusion.1), channel_id=2, replica_groups=mesh['gr'=2,'sp'=8,'tp'=2] {'sp'}, dimensions={0}, use_global_device_ids=true | all-gather | bytes 576 | tf_op jit(solution)/shard_map/all_gather | solution.py:9
  147.2 0.3 while.16
  147.5 5.0 %reduce-window.6 = f32[2,8,2,128]{3,1,2,0:T(8,128)S(1)} reduce-window(f32[2,8,2,128]{3,1,2,0:T(8,128)S(1)} %get-tuple-element.150, f32[]{:T(128)} %constant.72.clone.1), window={size=1x1x1x128 pad=0_0x0_0x0_0x0_127}, to_apply=%region_0.1 | reduce-window | flops 520192 | bytes 32772 | tf_op jit(solution)/shard_map/reduce-window
  152.5 0.1 slice_reduce_fusion
  152.6 1.0 copy.23
  153.6 0.1 fusion.17
  153.7 0.2 fusion.14
  153.9 17.9 %psum.7 = f32[2,8,64]{2,1,0:T(8,128)S(1)} all-reduce(f32[2,8,64]{2,1,0:T(8,128)S(1)} %bitcast.62), channel_id=1, replica_groups=mesh['gr'=2,'sp'=8,'tp'=2] {'sp'}, use_global_device_ids=true, to_apply=%region_5.6 | all-reduce | flops 1024 | bytes 8192 | tf_op jit(solution)/shard_map/psum | solution.py:82
  171.9 0.1 multiply_reduce_fusion
  172.0 0.1 broadcast_multiply_fusion
  172.1 0.7 reshape.53
  172.7 0.0 copy-done.1
  (14 shorter events, 0.2 us)
Async XLA Ops:
  7.2 7.9 %copy-start = (bf16[2,1024]{1,0:T(2,128)(2,1)S(1)}, bf16[2,1024]{1,0:T(2,128)(2,1)}, u32[]{:S(2)}) copy-start(bf16[2,1024]{1,0:T(2,128)(2,1)} %param.11) | copy-start | bytes 12292
  7.2 38.2 %all-gather.7.cloned.1.call-start = ((), (), s32[]{:S(2)}) async-start(), calls=%async_computation.2 | async-start | bytes 3145728 | tf_op jit(solution)/shard_map/all_gather | solution.py:48
  7.9 2.3 %copy-start.2 = (bf16[2,128,16]{1,2,0:T(8,128)(2,1)S(1)}, bf16[2,128,16]{1,2,0:T(8,128)(2,1)}, u32[]{:S(2)}) copy-start(bf16[2,128,16]{1,2,0:T(8,128)(2,1)} %param.13) | copy-start | bytes 24580
  7.9 7.2 %copy-start.3 = (f32[16]{0:T(128)S(1)}, f32[16]{0:T(128)}, u32[]{:S(2)}) copy-start(f32[16]{0:T(128)} %param.12) | copy-start | bytes 196
  7.9 114.7 %all-gather.5.cloned.1.call-start = ((), (), s32[]{:S(2)}) async-start(), calls=%async_computation.1 | async-start | bytes 4718592 | tf_op jit(solution)/shard_map/all_gather | solution.py:45
  10.8 118.4 %all-to-all-start = ((bf16[2,128,16]{1,0,2:T(2,128)(2,1)}), bf16[2,128,16]{1,0,2:T(2,128)(2,1)S(1)}, u32[]{:S(2)}, u32[]{:S(2)}) async-start(bf16[2,128,16]{1,0,2:T(2,128)(2,1)} %copy.20), calls=%async_computation | async-start | bytes 16384 | tf_op jit(solution)/shard_map/all_to_all | solution.py:54
  129.3 43.5 %copy-start.1 = (bf16[2,256,8]{1,2,0:T(8,128)(2,1)}, bf16[2,256,8]{1,2,0:T(8,128)(2,1)S(1)}, u32[]{:S(2)}) copy-start(bf16[2,256,8]{1,2,0:T(8,128)(2,1)S(1)} %get-tuple-element.151) | copy-start | bytes 24580
Sparse Core Ops, SparseCore 0:
  9.5 35.8 all-gather.6
  48.0 74.6 all-gather.4
where the time goes:
time: 180 us
  waiting for transfers between devices  108 us (60%)
  blocking collectives  35.7 us (20%)
  between operations  14.2 us (8%)
  other arithmetic  6.49 us (4%)
  matrix products  5.64 us (3%)
  local copies, waits for them, and re-layouts  4.99 us (3%)
  starting transfers between devices  4.31 us (2%)
    all_gather x1, waiting for transfers between devices, per_device(): full_cols = lax.all_gather(own_cols, 'sp', axis=0, tiled=True)  77.3 us
    all_gather x1, waiting for transfers between devices, per_device(): lax.all_gather(tokens, 'tp', axis=1, tiled=True)  30.2 us
    psum x1, blocking collectives, per_device(): mixture = lax.psum(partial_value, 'sp')  17.9 us
    all_gather x1, blocking collectives, carried_in(): everything = lax.all_gather(x, axis)  17.7 us
    dot_general x1, matrix products, per_device(): jnp.einsum('spd,dw->spw', lax.all_gather(tokens, 'tp', axis=1, tiled=True...  5.22 us
    another operation x2, other arithmetic  5.02 us
    all_to_all x1, starting transfers between devices, per_device(): lax.all_to_all(key_bias, 'tp', split_axis=2, concat_axis=1, tiled=True)  4.23 us
  transfers between devices with their start and end apart: 3, of which 2 were waited for; matrix products, arithmetic and copies ran while one was open for 5% of the time, Pallas kernels for 0%

commit v1 on v0

--- a/solution.py
+++ b/solution.py
@@ -79,7 +79,7 @@
     partial_value = jnp.einsum(
         "shp,sphc->shc", weights, value_blocks, preferred_element_type=jnp.float32
     )
-    mixture = lax.psum(partial_value, "sp")
+    mixture = jnp.sum(lax.all_gather(partial_value, "sp"), axis=0)
     reading = normalize(mixture).reshape(seq_count, col_width)
     return (key_cache, value_cache, bias_cache, reading)
 

time: 180 us -> 192 us (1.067)
  blocking collectives: 35.7 us -> 48.3 us
    all_gather x0 -> x1, blocking collectives: none -> 30.5 us  [per_device(): mixture = jnp.sum(lax.all_gather(partial_value, 'sp'), axis=0)]
    psum x1 -> x0, blocking collectives: 17.9 us -> none  [per_device(): mixture = lax.psum(partial_value, 'sp')]
where the time goes in v1:
time: 192 us
  waiting for transfers between devices  108 us (56%)
  blocking collectives  48.3 us (25%)
  between operations  14.2 us (7%)
  other arithmetic  6.51 us (3%)
  matrix products  5.64 us (3%)
  local copies, waits for them, and re-layouts  4.99 us (3%)
  starting transfers between devices  4.31 us (2%)
    all_gather x1, waiting for transfers between devices, per_device(): full_cols = lax.all_gather(own_cols, 'sp', axis=0, tiled=True)  77.3 us
    all_gather x1, blocking collectives, per_device(): mixture = jnp.sum(lax.all_gather(partial_value, 'sp'), axis=0)  30.5 us
    all_gather x1, waiting for transfers between devices, per_device(): lax.all_gather(tokens, 'tp', axis=1, tiled=True)  30.2 us
    all_gather x1, blocking collectives, carried_in(): everything = lax.all_gather(x, axis)  17.7 us
    dot_general x1, matrix products, per_device(): jnp.einsum('spd,dw->spw', lax.all_gather(tokens, 'tp', axis=1, tiled=True...  5.22 us
    another operation x2, other arithmetic  5.02 us
    all_to_all x1, starting transfers between devices, per_device(): lax.all_to_all(key_bias, 'tp', split_axis=2, concat_axis=1, tiled=True)  4.23 us
  transfers between devices with their start and end apart: 3, of which 2 were waited for; matrix products, arithmetic and copies ran while one was open for 5% of the time, Pallas kernels for 0%

profile of v1, /device:TPU:0, one launch (start us, length us, event | category | flops | bytes accessed | tf_op | source)
XLA Modules:
  0.0 192.2 jit_solution(868827216215149373)
XLA Ops:
  7.2 0.0 copy-start
  7.2 0.0 all-gather.8.cloned.1.call-start
  7.2 0.7 all-gather.8.cloned.1.call-update
  7.9 0.0 copy-start.2
  7.9 0.0 copy-start.3
  7.9 0.0 all-gather.6.cloned.1.call-start
  8.0 1.1 constant_dynamic-slice_fusion.1
  9.1 0.1 copy.28
  9.2 0.1 copy.29
  9.3 0.8 pad_maximum_fusion
  10.2 0.0 all-gather.6.cloned.1.call-update
  10.2 0.0 copy-done.2
  10.2 0.6 copy.20
  10.8 4.2 %all-to-all-start = ((bf16[2,128,16]{1,0,2:T(2,128)(2,1)}), bf16[2,128,16]{1,0,2:T(2,128)(2,1)S(1)}, u32[]{:S(2)}, u32[]{:S(2)}) async-start(bf16[2,128,16]{1,0,2:T(2,128)(2,1)} %copy.20), calls=%async_computation | async-start | bytes 16384 | tf_op jit(solution)/shard_map/all_to_all | solution.py:54
  15.0 0.0 copy-done
  15.1 0.1 reshape.65
  15.1 0.0 copy-done.3
  15.1 0.1 dynamic_slice.25
  15.2 30.2 %all-gather.8.cloned.1.call-done = bf16[2,256,2048]{2,1,0:T(8,128)(2,1)} async-done(((bf16[2,128,2048]{2,1,0:T(8,128)(2,1)}), bf16[2,256,2048]{2,1,0:T(8,128)(2,1)}) %all-gather.8.cloned.1.call-update) | async-done | bytes 2097168 | tf_op jit(solution)/shard_map/all_gather | solution.py:48
  45.4 77.3 %all-gather.6.cloned.1.call-done = bf16[2048,1024]{0,1:T(8,128)(2,1)} async-done(((bf16[256,1024]{0,1:T(8,128)(2,1)}), bf16[2048,1024]{0,1:T(8,128)(2,1)}) %all-gather.6.cloned.1.call-update) | async-done | bytes 4194320 | tf_op jit(solution)/shard_map/all_gather | solution.py:45
  122.7 5.2 %fusion.5 = bf16[2,256,1024]{1,2,0:T(8,128)(2,1)S(1)} fusion(bf16[2,256,2048]{2,1,0:T(8,128)(2,1)} %all-gather.8.cloned.1.call-done, bf16[2048,1024]{0,1:T(8,128)(2,1)} %all-gather.6.cloned.1.call-done), kind=kOutput, calls=%fused_computation.4 | convolution fusion | flops 2148007936 | bytes 7340032 | tf_op jit(solution)/shard_map/spd,dw->spw/dot_general | solution.py:46
  127.9 0.1 fusion.18
  128.0 0.2 fusion.19
  128.2 1.0 copy.22
  129.2 0.0 all-to-all-done
  129.2 0.1 negate_bitcast_fusion
  129.3 0.0 copy-start.1
  129.3 0.2 fusion.16
  129.5 17.7 %all-gather.2 = f32[8,2,8]{2,1,0:T(2,128)S(1)} all-gather(f32[1,2,8]{2,1,0:T(2,128)S(1)} %negate_bitcast_fusion.1), channel_id=2, replica_groups=mesh['gr'=2,'sp'=8,'tp'=2] {'sp'}, dimensions={0}, use_global_device_ids=true | all-gather | bytes 576 | tf_op jit(solution)/shard_map/all_gather | solution.py:9
  147.2 0.3 while.16
  147.5 5.0 %reduce-window.6 = f32[2,8,2,128]{3,1,2,0:T(8,128)S(1)} reduce-window(f32[2,8,2,128]{3,1,2,0:T(8,128)S(1)} %get-tuple-element.150, f32[]{:T(128)} %constant.72.clone.1), window={size=1x1x1x128 pad=0_0x0_0x0_0x0_127}, to_apply=%region_0.1 | reduce-window | flops 520192 | bytes 32772 | tf_op jit(solution)/shard_map/reduce-window
  152.5 0.1 slice_reduce_fusion
  152.6 1.0 copy.23
  153.6 0.1 fusion.17
  153.7 0.2 fusion.14
  153.9 30.5 %all-gather.1 = f32[16,8,64]{2,1,0:T(8,128)S(1)} all-gather(f32[2,8,64]{2,1,0:T(8,128)S(1)} %bitcast.64), channel_id=3, replica_groups=mesh['gr'=2,'sp'=8,'tp'=2] {'sp'}, dimensions={0}, use_global_device_ids=true | all-gather | bytes 36864 | tf_op jit(solution)/shard_map/all_gather | solution.py:82
  184.5 0.1 multiply_reduce_fusion
  184.6 0.1 broadcast_multiply_fusion
  184.7 0.7 mul.34
  185.4 0.0 copy-done.1
  (15 shorter events, 0.2 us)
Async XLA Ops:
  7.2 7.9 %copy-start = (bf16[2,1024]{1,0:T(2,128)(2,1)S(1)}, bf16[2,1024]{1,0:T(2,128)(2,1)}, u32[]{:S(2)}) copy-start(bf16[2,1024]{1,0:T(2,128)(2,1)} %param.11) | copy-start | bytes 12292
  7.2 38.2 %all-gather.8.cloned.1.call-start = ((), (), s32[]{:S(2)}) async-start(), calls=%async_computation.2 | async-start | bytes 3145728 | tf_op jit(solution)/shard_map/all_gather | solution.py:48
  7.9 2.3 %copy-start.2 = (bf16[2,128,16]{1,2,0:T(8,128)(2,1)S(1)}, bf16[2,128,16]{1,2,0:T(8,128)(2,1)}, u32[]{:S(2)}) copy-start(bf16[2,128,16]{1,2,0:T(8,128)(2,1)} %param.13) | copy-start | bytes 24580
  7.9 7.2 %copy-start.3 = (f32[16]{0:T(128)S(1)}, f32[16]{0:T(128)}, u32[]{:S(2)}) copy-start(f32[16]{0:T(128)} %param.12) | copy-start | bytes 196
  7.9 114.7 %all-gather.6.cloned.1.call-start = ((), (), s32[]{:S(2)}) async-start(), calls=%async_computation.1 | async-start | bytes 4718592 | tf_op jit(solution)/shard_map/all_gather | solution.py:45
  10.8 118.4 %all-to-all-start = ((bf16[2,128,16]{1,0,2:T(2,128)(2,1)}), bf16[2,128,16]{1,0,2:T(2,128)(2,1)S(1)}, u32[]{:S(2)}, u32[]{:S(2)}) async-start(bf16[2,128,16]{1,0,2:T(2,128)(2,1)} %copy.20), calls=%async_computation | async-start | bytes 16384 | tf_op jit(solution)/shard_map/all_to_all | solution.py:54
  129.3 56.1 %copy-start.1 = (bf16[2,256,8]{1,2,0:T(8,128)(2,1)}, bf16[2,256,8]{1,2,0:T(8,128)(2,1)S(1)}, u32[]{:S(2)}) copy-start(bf16[2,256,8]{1,2,0:T(8,128)(2,1)S(1)} %get-tuple-element.151) | copy-start | bytes 24580
Sparse Core Ops, SparseCore 0:
  9.5 35.8 all-gather.7
  48.0 74.6 all-gather.5
